TPU v7x, 32 devices: a whole 2x2x4 slice. The times are simulated.
32 devices in a mesh: grp: 2 (over y), sp: 4 (over z), dp: 4 (over x, core).
Axes of the slice: x: 2, y: 2, z: 4, core: 2. Of those that a mesh axis runs over, the one named last changes fastest.
Arguments:
- gate_input: bfloat16 [8, 1536, 2048], P(('grp', 'dp'), 'sp'), parts along dimension 0, may hold values from -6 to 6
- value_input: bfloat16 [8, 1536, 2048], P(('grp', 'dp'), 'sp'), parts along dimension 0, may hold values from -6 to 6
- norm_gain: bfloat16 [2048], replicated, may hold values from 0.099609375 to 1.8984375
- norm_bias: bfloat16 [2048], replicated, may hold values from -2.5 to 2.5
- mix_weight: bfloat16 [16, 1024, 1024], P('sp', 'dp'), may hold values from -0.1875 to 0.1875
- mix_bias: bfloat16 [16, 1024], P('sp'), may hold values from 0.099609375 to 1.8984375
Outputs:
- gated: bfloat16 [8, 1536, 2048], P(('grp', 'dp'), 'sp'), parts along dimension 0
There are 2 independent parts, one for each index of `grp`. A program takes and returns all parts, laid end to end along the dimension named above; an argument that names none is the same for every part. Nothing has to cross between parts.
All inputs are finite; a program needn't handle non-finite values.
Results may differ from a plain program's by a relative error of at most 0.0053.
Values may be sent and summed in bfloat16 or wider, within the bound.
A program may use at most 64 MiB of HBM per device.

v0:
```python
import jax
import jax.numpy as jnp
from jax import lax
from jax.sharding import PartitionSpec as P

GD = 128
BLK = 1024


def mix_groups(normed_ex, mix_weight, mix_bias):
    seqs, length, local_width = normed_ex.shape
    groups_here = mix_weight.shape[0]
    nblocks = -(-length // BLK)
    padded = jnp.pad(normed_ex, ((0, 0), (0, nblocks * BLK - length), (0, 0)))
    blocks = padded.reshape(seqs * nblocks, BLK, groups_here, GD)
    piece = lax.all_gather(mix_weight, "dp", axis=1, tiled=True)
    count = piece.shape[1]
    rows = lax.iota(jnp.int32, count)
    cols = lax.iota(jnp.int32, BLK)
    keep = cols[None, :] <= rows[:, None]
    masked = jnp.where(keep[None], piece, jnp.zeros_like(piece))
    term = jnp.einsum("gts,bsgc->btgc", masked, blocks, preferred_element_type=jnp.float32)
    bias_rows = mix_bias.astype(jnp.float32)
    mixed = term + bias_rows.T[None, :, :, None]
    mixed = mixed.reshape(seqs, nblocks * BLK, local_width)[:, :length]
    return mixed.astype(jnp.bfloat16)


def body(gate_input, value_input, norm_gain, norm_bias, mix_weight, mix_bias):
    act = jax.nn.gelu(value_input.astype(jnp.float32))
    mean = jnp.mean(act, axis=-1, keepdims=True)
    var = jnp.mean(jnp.square(act - mean), axis=-1, keepdims=True)
    normed = (
        (act - mean) * lax.rsqrt(var + 1e-06) * norm_gain.astype(jnp.float32)
        + norm_bias.astype(jnp.float32)
    ).astype(jnp.bfloat16)
    normed_ex = lax.all_to_all(normed, "sp", split_axis=2, concat_axis=1, tiled=True)
    mixed = mix_groups(normed_ex, mix_weight, mix_bias)
    returned = lax.all_to_all(mixed, "sp", split_axis=1, concat_axis=2, tiled=True)
    gated = jax.nn.gelu(gate_input.astype(jnp.float32)) * returned.astype(jnp.float32)
    return gated.astype(jnp.bfloat16)


def solution(mesh):
    placed = (
        P(("grp", "dp"), "sp", None),
        P(("grp", "dp"), "sp", None),
        P(),
        P(),
        P("sp", "dp", None),
        P("sp", None),
    )
    return jax.shard_map(
        body, mesh=mesh, in_specs=placed, out_specs=P(("grp", "dp"), "sp", None), check_vma=False
    )
```

profile of v0, /device:TPU:0, one launch (start us, length us, event | category | flops | bytes accessed | tf_op | source)
XLA Modules:
  0.0 239.9 jit_solution(9603832664579578522)
XLA Ops:
  6.5 0.0 copy-start
  6.5 0.0 copy-start.4
  6.5 0.0 copy-start.5
  6.5 0.0 all-gather.2.cloned.1.call-start
  6.5 0.7 all-gather.2.cloned.1.call-update
  7.3 0.7 copy-done
  7.9 0.9 copy.17
  8.8 0.0 copy-done.4
  8.8 0.0 copy-done.5
  8.8 1.1 fusion.23
  10.0 1.3 multiply_reduce_fusion
  11.3 1.5 add_convert_fusion
  12.9 30.1 %copy.35 = bf16[1,384,2048]{1,0,2:T(2,128)(2,1)S(1)} copy(bf16[1,384,2048]{1,2,0:T(8,128)(2,1)S(1)} %add_convert_fusion) | data formatting | bytes 3145728 | tf_op jit(solution)/shard_map/convert_element_type | solution.py:36
  43.0 0.5 broadcast.85
  43.5 34.4 %reduce.2 = bf16[2048,384]{1,0:T(8,128)(2,1)} reduce(bf16[2048,1,384]{2,1,0:T(2,128)(2,1)S(1)} %bitcast.31, bf16[]{:T(256)} %broadcast.85), dimensions={1}, to_apply=%bitcast.30.reduce_sub_computation | reduce | bytes 3145730
  77.9 0.0 copy-start.3
  77.9 3.7 %reshape.69 = bf16[4,2,98304]{2,1,0:T(2,128)(2,1)} reshape(bf16[2048,384]{1,0:T(8,128)(2,1)} %reduce.2) | data formatting | bytes 3145728
  81.7 6.3 %all-to-all-start = ((bf16[4,2,98304]{2,1,0:T(2,128)(2,1)}), bf16[4,2,98304]{2,1,0:T(2,128)(2,1)}, u32[]{:S(2)}, u32[]{:S(2)}) async-start(bf16[4,2,98304]{2,1,0:T(2,128)(2,1)} %reshape.69), calls=%async_computation | async-start | bytes 3145728 | tf_op jit(solution)/shard_map/all_to_all | solution.py:37
  88.0 1.3 iota_compare_fusion
  89.3 0.0 copy-done.3
  89.3 35.8 %all-to-all-done = bf16[4,2,98304]{2,1,0:T(2,128)(2,1)} async-done(((bf16[4,2,98304]{2,1,0:T(2,128)(2,1)}), bf16[4,2,98304]{2,1,0:T(2,128)(2,1)}, u32[]{:S(2)}, u32[]{:S(2)}) %all-to-all-start) | async-done | bytes 1572896 | tf_op jit(solution)/shard_map/all_to_all | solution.py:37
  125.1 3.1 %reshape.70 = bf16[2048,1,384]{2,1,0:T(2,128)(2,1)S(1)} reshape(bf16[4,2,98304]{2,1,0:T(2,128)(2,1)} %all-to-all-done) | data formatting | bytes 3145728
  128.2 1.4 copy.27
  129.6 2.6 %copy.19 = bf16[1,4,384,512]{3,2,1,0:T(8,128)(2,1)} copy(bf16[1,4,384,512]{2,3,1,0:T(8,128)(2,1)} %bitcast.36) | data formatting | bytes 3145728 | tf_op jit(solution)/shard_map/all_to_all | solution.py:37
  132.2 0.0 copy-start.2
  132.2 1.6 pad.4
  133.8 2.1 reshape.64
  135.9 0.0 all-gather.2.cloned.1.call-done
  135.9 0.0 copy-done.2
  135.9 8.1 %fusion.4 = bf16[2,1024,4,128]{1,3,0,2:T(8,128)(2,1)} fusion(f32[1024,4]{0,1:T(4,128)S(1)} %convert_bitcast_fusion.1, bf16[4,1024,1024]{2,1,0:T(8,128)(2,1)} %all-gather.2.cloned.1.call-done, pred[1024,1024]{1,0:T(8,128)(4,1)S(1)} %copy-done.2, bf16[2,1024,4,128]{3,2,1,0:T(4,128)(2,1)} %reshape.64), kind=kOutput, calls=%fused_computation.13 | convolution fusion | flops 2153775104 | bytes 13647872 | tf_op jit(solution)/shard_map/gts,bsgc->btgc/dot_general | solution.py:22
  144.0 3.1 %copy.21 = bf16[2,1024,4,128]{3,2,1,0:T(4,128)(2,1)S(1)} copy(bf16[2,1024,4,128]{1,3,0,2:T(8,128)(2,1)} %fusion.4) | data formatting | bytes 4194304 | tf_op jit(solution)/shard_map/convert.5
  147.2 2.2 reshape.65
  149.4 0.0 slice-start
  149.4 1.4 slice-done
  150.8 11.7 %copy.34 = bf16[1,1536,512]{2,0,1:T(2,128)(2,1)S(1)} copy(bf16[1,1536,512]{2,1,0:T(8,128)(2,1)S(1)} %slice-done) | data formatting | bytes 3145728 | tf_op jit(solution)/shard_map/slice | solution.py:25
  162.5 11.1 %reduce.3 = bf16[1536,512]{1,0:T(8,128)(2,1)} reduce(bf16[1536,1,512]{2,1,0:T(2,128)(2,1)S(1)} %bitcast.32, bf16[]{:T(256)} %broadcast.85), dimensions={1}, to_apply=%bitcast.29.reduce_sub_computation | reduce | bytes 3145730
  173.5 0.0 copy-start.1
  173.5 4.3 %reshape.71 = bf16[4,2,98304]{2,1,0:T(2,128)(2,1)} reshape(bf16[1536,512]{1,0:T(8,128)(2,1)} %reduce.3) | data formatting | bytes 3145728
  177.8 4.3 %all-to-all-start.1 = ((bf16[4,2,98304]{2,1,0:T(2,128)(2,1)}), bf16[4,2,98304]{2,1,0:T(2,128)(2,1)}, u32[]{:S(2)}, u32[]{:S(2)}) async-start(bf16[4,2,98304]{2,1,0:T(2,128)(2,1)} %reshape.71), calls=%async_computation.1 | async-start | bytes 3145728 | tf_op jit(solution)/shard_map/all_to_all | solution.py:39
  182.1 0.0 copy-done.1
  182.2 1.6 copy.16
  183.7 35.0 %all-to-all-done.1 = bf16[4,2,98304]{2,1,0:T(2,128)(2,1)} async-done(((bf16[4,2,98304]{2,1,0:T(2,128)(2,1)}), bf16[4,2,98304]{2,1,0:T(2,128)(2,1)}, u32[]{:S(2)}, u32[]{:S(2)}) %all-to-all-start.1) | async-done | bytes 1572896 | tf_op jit(solution)/shard_map/all_to_all | solution.py:39
  218.7 3.1 %reshape.72 = bf16[1536,1,512]{2,1,0:T(2,128)(2,1)S(1)} reshape(bf16[4,2,98304]{2,1,0:T(2,128)(2,1)} %all-to-all-done.1) | data formatting | bytes 3145728
  221.8 0.4 copy.23
  222.2 2.1 convert_bitcast_fusion
  224.3 2.4 copy.24
  226.7 3.8 %fusion.12 = bf16[1,384,2048]{1,2,0:T(8,128)(2,1)} fusion(bf16[1,384,2048]{1,2,0:T(8,128)(2,1)} %copy.16, f32[1,384,4,512]{1,3,2,0:T(8,128)S(1)} %copy.24), kind=kLoop, calls=%fused_computation.22 | loop fusion | flops 8650752 | bytes 6291456 | tf_op jit(solution)/shard_map/convert_element_type | solution.py:41
  230.5 2.6 %copy.25 = bf16[1,384,2048]{2,1,0:T(8,128)(2,1)} copy(bf16[1,384,2048]{1,2,0:T(8,128)(2,1)} %fusion.12) | data formatting | bytes 3145728 | tf_op jit(solution)/shard_map/convert_element_type | solution.py:41
  (5 shorter events, 0.0 us)
Async XLA Ops:
  6.5 1.4 copy-start
  6.5 2.3 copy-start.4
  6.5 2.3 copy-start.5
  6.5 129.4 %all-gather.2.cloned.1.call-start = ((), (), s32[]{:S(2)}) async-start(), calls=%async_computation.2 | async-start | bytes 10485760 | tf_op jit(solution)/shard_map/all_gather | solution.py:16
  77.9 11.4 %copy-start.3 = (bf16[4,1024]{1,0:T(4,128)(2,1)S(1)}, bf16[4,1024]{1,0:T(4,128)(2,1)}, u32[]{:S(2)}) copy-start(bf16[4,1024]{1,0:T(4,128)(2,1)} %param.11) | copy-start | bytes 24580
  81.7 43.4 %all-to-all-start = ((bf16[4,2,98304]{2,1,0:T(2,128)(2,1)}), bf16[4,2,98304]{2,1,0:T(2,128)(2,1)}, u32[]{:S(2)}, u32[]{:S(2)}) async-start(bf16[4,2,98304]{2,1,0:T(2,128)(2,1)} %reshape.69), calls=%async_computation | async-start | bytes 3145728 | tf_op jit(solution)/shard_map/all_to_all | solution.py:37
  132.2 3.7 %copy-start.2 = (pred[1024,1024]{1,0:T(8,128)(4,1)S(1)}, pred[1024,1024]{1,0:T(8,128)(4,1)}, u32[]{:S(2)}) copy-start(pred[1024,1024]{1,0:T(8,128)(4,1)} %iota_compare_fusion) | copy-start | bytes 3145732
  149.4 1.4 slice-start
  173.5 8.6 %copy-start.1 = (bf16[1,384,2048]{2,1,0:T(8,128)(2,1)S(1)}, bf16[1,384,2048]{2,1,0:T(8,128)(2,1)}, u32[]{:S(2)}) copy-start(bf16[1,384,2048]{2,1,0:T(8,128)(2,1)} %param.6) | copy-start | bytes 4718596
  177.8 40.9 %all-to-all-start.1 = ((bf16[4,2,98304]{2,1,0:T(2,128)(2,1)}), bf16[4,2,98304]{2,1,0:T(2,128)(2,1)}, u32[]{:S(2)}, u32[]{:S(2)}) async-start(bf16[4,2,98304]{2,1,0:T(2,128)(2,1)} %reshape.71), calls=%async_computation.1 | async-start | bytes 3145728 | tf_op jit(solution)/shard_map/all_to_all | solution.py:39
Sparse Core Ops, SparseCore 0:
  8.9 60.9 all-gather.1
where the time goes:
time: 241 us; the launch traced here: 240 us
  local copies, waits for them, and re-layouts  79.4 us (33%)
  waiting for transfers between devices  71.5 us (30%)
  other arithmetic  56.7 us (24%)
  between operations  13.5 us (6%)
  starting transfers between devices  10.7 us (4%)
  matrix products  8.09 us (3%)
    unnamed x2, other arithmetic  45.5 us
    all_to_all x1, waiting for transfers between devices, body(): lax.all_to_all(normed, 'sp', split_axis=2, concat_axis=1, tiled=True)  35.8 us
    all_to_all x1, waiting for transfers between devices, body(): lax.all_to_all(mixed, 'sp', split_axis=1, concat_axis=2, tiled=True)  35 us
    convert_element_type x1, local copies, waits for them, and re-layouts, body(): normed = ((act - mean) * lax.rsqrt(var + 1e-06) * norm_gain.astype(jnp.fl...  30.1 us
    unnamed x20, local copies, waits for them, and re-layouts  19.2 us
    slice x3, local copies, waits for them, and re-layouts, mix_groups(): mixed = mixed.reshape(seqs, nblocks * BLK, local_width)[:, :length]  13.1 us
    dot_general x1, matrix products, mix_groups(): jnp.einsum('gts,bsgc->btgc', masked, blocks, preferred_element_type=jnp.f...  8.09 us
    all_to_all x1, starting transfers between devices, body(): lax.all_to_all(normed, 'sp', split_axis=2, concat_axis=1, tiled=True)  6.35 us
  transfers between devices with their start and end apart: 3, of which 2 were waited for; matrix products, arithmetic and copies ran while one was open for 36% of the time, Pallas kernels for 0%

commit v1 on v0

v1 whole, which is shorter than its diff:
```python
import functools

import jax
import jax.numpy as jnp
from jax import lax
from jax.experimental import pallas as pl
from jax.experimental.pallas import tpu as pltpu
from jax.sharding import PartitionSpec as P

GD = 128
BLK = 1024
ROOT_2_PI = 0.7978845608028654


def gelu(x):
    return (0.5 * x) * (1.0 + jnp.tanh(ROOT_2_PI * (x + 0.044715 * (x * x * x))))


def segments(dest, span):
    runs, at = [], dest * span
    while at < (dest + 1) * span:
        stop = min((dest + 1) * span, (at // BLK + 1) * BLK)
        runs.append((at, stop))
        at = stop
    return runs


def kernel(
    ngrp, nsp, ndp, value_hbm, gate_hbm, gain_ref, nbias_ref, w_hbm, mbias_ref, out_ref,
    vbuf, gbuf, ggelu, nsend, ex, rsend, ret, wbuf,
    v_sem, g_sem, w_sem, own_sem, ret_own_sem,
    f_ssem, f_rsem, b_ssem, b_rsem,
    o_ssem, o_rsem, x_ssem, x_rsem, y_ssem, y_rsem, c_ssem, c_rsem,
):
    span, width = vbuf.shape
    cw = width // nsp
    groups = cw // GD
    piece = v_piece(span)
    pieces = span // piece
    nx = ndp // 2
    rows = BLK // ndp
    part = rows // ngrp
    p, z, r = lax.axis_index("grp"), lax.axis_index("sp"), lax.axis_index("dp")
    xi, core = r // 2, r % 2
    mate = r + 1 - 2 * core

    def value_copy(i):
        at = pl.ds(i * piece, piece)
        return pltpu.make_async_copy(value_hbm.at[0, at], vbuf.at[at], v_sem.at[i])

    def own_rows(block, q, count):
        return pl.ds(pl.multiple_of(block * rows + q * part, part), count)

    mine = own_rows(r, 0, rows)
    w_copy = pltpu.make_async_copy(w_hbm, wbuf.at[:, mine], w_sem)
    gate_copy = pltpu.make_async_copy(gate_hbm.at[0], gbuf, g_sem)
    value_copy(0).start()
    w_copy.start()
    for i in range(1, pieces):
        value_copy(i).start()
    gate_copy.start()

    barrier = pltpu.get_barrier_semaphore()
    peers = [{"sp": lax.rem(z + k, nsp)} for k in range(1, nsp)]
    peers += [{"dp": mate}]
    peers += [{"dp": lax.rem(xi + k, nx) * 2 + core} for k in range(1, nx)]
    peers += [{"grp": lax.rem(p + k, ngrp)} for k in range(1, ngrp)]
    for peer in peers:
        pl.semaphore_signal(barrier, inc=1, device_id=peer, device_id_type=pl.DeviceIdType.MESH)
    pl.semaphore_wait(barrier, len(peers))

    def remote(src, dst, ssem, rsem, device):
        return pltpu.make_async_remote_copy(
            src_ref=src, dst_ref=dst, send_sem=ssem, recv_sem=rsem,
            device_id=device, device_id_type=pl.DeviceIdType.MESH,
        )

    upper = z // ((nsp + 1) // 2)

    def peer_at(j):
        return upper * j + (1 - upper) * (nsp - 1 - j)

    def ex_rows(src, i):
        return pl.ds(pl.multiple_of(src * span + i * piece, piece), piece)

    def forward(i, dest, src):
        return remote(
            nsend.at[dest, pl.ds(i * piece, piece)], ex.at[ex_rows(src, i)],
            f_ssem.at[i, dest], f_rsem.at[i, src], {"sp": dest},
        )

    def forward_own(i):
        return pltpu.make_async_copy(
            nsend.at[z, pl.ds(i * piece, piece)], ex.at[ex_rows(z, i)], own_sem.at[i]
        )

    gain = gain_ref[...].astype(jnp.float32)
    nbias = nbias_ref[...].astype(jnp.float32)

    def normalise(i):
        def step(s, carry):
            at = pl.ds(pl.multiple_of(i * piece + s * 16, 16), 16)
            act = gelu(vbuf[at, :].astype(jnp.float32))
            mean = jnp.sum(act, axis=-1, keepdims=True) * (1.0 / width)
            act = act - mean
            var = jnp.sum(act * act, axis=-1, keepdims=True) * (1.0 / width)
            normed = (act * lax.rsqrt(var + 1e-06) * gain + nbias).astype(jnp.bfloat16)
            for t in range(nsp):
                nsend[t, at, :] = normed[:, t * cw:(t + 1) * cw]
            return carry

        lax.fori_loop(0, piece // 16, step, 0, unroll=2)

    def w_own():
        return remote(wbuf.at[:, mine], wbuf.at[:, mine], o_ssem, o_rsem, {"dp": mate})

    def w_own_in():
        at = own_rows(mate, 0, rows)
        return remote(wbuf.at[:, at], wbuf.at[:, at], o_ssem, o_rsem, {"dp": mate})

    def w_x(g, src, dest, slot):
        at = wbuf.at[g, own_rows(src * 2 + core, p, part)]
        return remote(at, at, x_ssem.at[slot, g], x_rsem.at[src, g], {"dp": dest * 2 + core})

    def w_y(g, src, q, slot, dest):
        at = wbuf.at[g, own_rows(src * 2 + core, q, part)]
        return remote(at, at, y_ssem.at[slot, src, g], y_rsem.at[q, src, g], {"grp": dest})

    def w_c(g, src, q, side):
        at = wbuf.at[g, own_rows(src * 2 + side, q, part)]
        return remote(at, at, c_ssem.at[q, src, g], c_rsem.at[q, src, g], {"dp": mate})

    for i in range(pieces):
        value_copy(i).wait()
        normalise(i)
        forward_own(i).start()
        for j in range(nsp):
            dest = peer_at(j)

            @pl.when(dest != z)
            def _(i=i, dest=dest):
                forward(i, dest, z).start()

        if i == 0:
            w_copy.wait()
            for g in range(groups):
                for k in range(1, nx):
                    w_x(g, xi, lax.rem(xi + k, nx), k - 1).start()
            w_own().start()

    def from_y(g):
        for k in range(1, nx):
            src = lax.rem(xi + nx - k, nx)
            for m in range(1, ngrp):
                q = lax.rem(p + ngrp - m, ngrp)
                w_y(g, src, q, m - 1, q).wait_recv()
                w_c(g, src, q, core).start()

    for g in range(groups):
        for k in range(1, nx):
            src = lax.rem(xi + nx - k, nx)
            w_x(g, src, src, k - 1).wait_recv()
            for m in range(1, ngrp):
                w_y(g, src, p, m - 1, lax.rem(p + m, ngrp)).start()
            w_c(g, src, p, core).start()
        if g == 0:
            gate_copy.wait()

            def gate_step(s, carry):
                at = pl.ds(pl.multiple_of(s * 16, 16), 16)
                ggelu[at, :] = gelu(gbuf[at, :].astype(jnp.float32))
                return carry

            lax.fori_loop(0, span // 16, gate_step, 0)
        else:
            from_y(g - 1)
    from_y(groups - 1)
    w_own_in().wait_recv()
    for g in range(groups):
        for k in range(1, nx):
            src = lax.rem(xi + k, nx)
            for q in range(ngrp):
                w_c(g, src, q, 1 - core).wait_recv()

    ready = set()

    def need(src):
        if src in ready:
            return
        ready.add(src)

        @pl.when(z == src)
        def _():
            for i in range(pieces):
                forward_own(i).wait()

        @pl.when(z != src)
        def _():
            for i in range(pieces):
                forward(i, src, src).wait_recv()

    def back(dest, src):
        return remote(
            rsend.at[dest], ret.at[src], b_ssem.at[dest], b_rsem.at[src], {"sp": dest}
        )

    def back_own():
        return pltpu.make_async_copy(rsend.at[z], ret.at[z], ret_own_sem)

    order = []
    for j in range((nsp + 1) // 2):
        order += [j] if j == nsp - 1 - j else [j, nsp - 1 - j]
    for dest in order:
        for at, stop in segments(dest, span):
            base = at // BLK * BLK
            t0, size = at - base, stop - at
            for src in range(base // span, (stop - 1) // span + 1):
                need(src)
            keep = (
                lax.broadcasted_iota(jnp.int32, (size, size), 1)
                <= lax.broadcasted_iota(jnp.int32, (size, size), 0)
            )
            for g in range(groups):
                lanes = slice(g * GD, (g + 1) * GD)
                diag = wbuf[g, t0:t0 + size, t0:t0 + size]
                diag = jnp.where(keep, diag, jnp.zeros_like(diag))
                acc = jnp.dot(diag, ex[at:stop, lanes], preferred_element_type=jnp.float32)
                if t0:
                    acc += jnp.dot(
                        wbuf[g, t0:t0 + size, :t0], ex[base:at, lanes],
                        preferred_element_type=jnp.float32,
                    )
                acc += mbias_ref[t0:t0 + size, g:g + 1]
                rsend[dest, at - dest * span:stop - dest * span, lanes] = acc.astype(jnp.bfloat16)

        @pl.when(z == dest)
        def _():
            back_own().start()

        @pl.when(z != dest)
        def _():
            back(dest, z).start()

    def gate_out(src):
        lanes = pl.ds(pl.multiple_of(src * cw, GD), cw)

        def step(s, carry):
            at = pl.ds(pl.multiple_of(s * 16, 16), 16)
            out_ref[0, at, lanes] = (
                ggelu[at, lanes] * ret[src, at, :].astype(jnp.float32)
            ).astype(jnp.bfloat16)
            return carry

        lax.fori_loop(0, span // 16, step, 0, unroll=2)

    back_own().wait()
    gate_out(z)
    for j in reversed(range(nsp)):
        src = peer_at(j)

        @pl.when(src != z)
        def _(src=src):
            back(src, src).wait_recv()
            gate_out(src)

    for j in range(nsp):
        dest = peer_at(j)

        @pl.when(dest != z)
        def _(dest=dest):
            for i in range(pieces):
                forward(i, dest, z).wait_send()
            back(dest, z).wait_send()

    w_own().wait_send()
    for g in range(groups):
        for k in range(1, nx):
            w_x(g, xi, lax.rem(xi + k, nx), k - 1).wait_send()
            src = lax.rem(xi + k, nx)
            for m in range(1, ngrp):
                w_y(g, src, p, m - 1, lax.rem(p + m, ngrp)).wait_send()
            for q in range(ngrp):
                w_c(g, src, q, core).wait_send()


def v_piece(span):
    return 128 if span % 128 == 0 else span


def body(ngrp, nsp, ndp, gate_input, value_input, norm_gain, norm_bias, mix_weight, mix_bias):
    _, span, width = value_input.shape
    groups = mix_weight.shape[0]
    cw = groups * GD
    pieces = span // v_piece(span)
    nx = ndp // 2
    dma = pltpu.SemaphoreType.DMA
    bf16, f32 = jnp.bfloat16, jnp.float32
    vmem, hbm = pl.BlockSpec(memory_space=pltpu.VMEM), pl.BlockSpec(memory_space=pl.ANY)
    return pl.pallas_call(
        functools.partial(kernel, ngrp, nsp, ndp),
        out_shape=jax.ShapeDtypeStruct(value_input.shape, bf16),
        in_specs=[hbm, hbm, vmem, vmem, hbm, vmem],
        out_specs=vmem,
        scratch_shapes=[
            pltpu.VMEM((span, width), bf16),
            pltpu.VMEM((span, width), bf16),
            pltpu.VMEM((span, width), f32),
            pltpu.VMEM((nsp, span, cw), bf16),
            pltpu.VMEM((nsp * span, cw), bf16),
            pltpu.VMEM((nsp, span, cw), bf16),
            pltpu.VMEM((nsp, span, cw), bf16),
            pltpu.VMEM((groups, BLK, BLK), bf16),
            dma((pieces,)), dma, dma, dma((pieces,)), dma,
            dma((pieces, nsp)), dma((pieces, nsp)), dma((nsp,)), dma((nsp,)),
            dma, dma,
            dma((max(nx - 1, 1), groups)), dma((nx, groups)),
            dma((max(ngrp - 1, 1), nx, groups)), dma((ngrp, nx, groups)),
            dma((ngrp, nx, groups)), dma((ngrp, nx, groups)),
        ],
        compiler_params=pltpu.CompilerParams(
            collective_id=0, has_side_effects=True, vmem_limit_bytes=50 * 1024 * 1024
        ),
    )(
        value_input, gate_input, norm_gain[None], norm_bias[None], mix_weight,
        mix_bias.astype(f32).T,
    )


def solution(mesh):
    placed = (
        P(("grp", "dp"), "sp", None),
        P(("grp", "dp"), "sp", None),
        P(),
        P(),
        P("sp", "dp", None),
        P("sp", None),
    )
    return jax.shard_map(
        functools.partial(body, mesh.shape["grp"], mesh.shape["sp"], mesh.shape["dp"]),
        mesh=mesh, in_specs=placed, out_specs=P(("grp", "dp"), "sp", None), check_vma=False,
    )
```

time: 241 us -> 87.3 us (0.36)
  the two profiles are of different devices: /device:TPU:0 before, /device:TPU:23 now
where the time goes in v1:
time: 87.3 us; the launch traced here: 87 us
  Pallas kernels  82.2 us (94%)
  local copies, waits for them, and re-layouts  4.8 us (5%)
    pallas_call x1, Pallas kernels, body(): pl.pallas_call(functools.partial(kernel, ngrp, nsp, ndp), out_shape=jax.S...  82.2 us
    unnamed x3, local copies, waits for them, and re-layouts  2.55 us

profile of v1, /device:TPU:23, one launch (start us, length us, event | category | flops | bytes accessed | tf_op | source)
XLA Modules:
  0.0 87.0 jit_solution(2025216350143179958)
XLA Ops:
  0.0 0.7 broadcast_in_dim.6.gain_ref
  0.7 0.7 broadcast_in_dim.7.nbias_ref
  1.4 0.9 copy.7
  2.3 0.0 copy-start
  2.3 1.4 %copy-done = bf16[1,384,2048]{2,1,0:T(8,128)(2,1)S(1)} copy-done((bf16[1,384,2048]{2,1,0:T(8,128)(2,1)S(1)}, bf16[1,384,2048]{2,1,0:T(8,128)(2,1)}, u32[]{:S(2)}) %copy-start) | copy-done | bytes 1572888
  3.7 82.2 %shard_map.64 = bf16[1,384,2048]{2,1,0:T(8,128)(2,1)S(1)} custom-call(bf16[1,384,2048]{2,1,0:T(8,128)(2,1)S(1)} %copy-done, bf16[1,384,2048]{2,1,0:T(8,128)(2,1)} %gate_hbm.1, bf16[1,2048]{1,0:T(2,128)(2,1)S(1)} %broadcast_in_dim.6.gain_ref, bf16[1,2048]{1,0:T(2,128)(2,1)S(1)} %broadcast_in_dim.7.nbias_ref, bf16[4,256,1024]{2,1,0:T(8,128)(2,1)} %w_hbm.1, ...), custom_call_target="tpu_custom_call" | custom-call | tf_op jit(solution)/shard_map/pallas_call | solution.py:299
  85.9 1.1 %copy.9 = bf16[1,384,2048]{2,1,0:T(8,128)(2,1)} copy(bf16[1,384,2048]{2,1,0:T(8,128)(2,1)S(1)} %shard_map.64) | data formatting | bytes 3145728
Async XLA Ops:
  2.3 1.4 %copy-start = (bf16[1,384,2048]{2,1,0:T(8,128)(2,1)S(1)}, bf16[1,384,2048]{2,1,0:T(8,128)(2,1)}, u32[]{:S(2)}) copy-start(bf16[1,384,2048]{2,1,0:T(8,128)(2,1)} %value_hbm.1) | copy-start | bytes 4718596

commit v2 on v1

v2 whole, which is shorter than its diff:
```python
import functools

import jax
import jax.numpy as jnp
from jax import lax
from jax.experimental import pallas as pl
from jax.experimental.pallas import tpu as pltpu
from jax.sharding import PartitionSpec as P

GD = 128
BLK = 1024
ROOT_2_PI = 0.7978845608028654


def gelu(x):
    return (0.5 * x) * (1.0 + jnp.tanh(ROOT_2_PI * (x + 0.044715 * (x * x * x))))


def guest_rows(ngrp, nsp, ndp, span):
    length, rows = nsp * span, BLK // ndp
    tail = length - BLK
    fits = nsp % 2 == 0 and ndp == 4 and ngrp == 2 and tail == 2 * rows
    return tail if fits and 2 * tail <= length and v_piece(span) == 128 else 0


def kernel(
    ngrp, nsp, ndp, value_hbm, gate_hbm, gain_ref, nbias_ref, w_hbm, mbias_ref, out_ref,
    vbuf, gbuf, ggelu, nsend, ex, rsend, ret, wbuf, wguest,
    v_sem, g_sem, w_sem, own_sem, ret_own_sem,
    f_ssem, f_rsem, b_ssem, b_rsem,
    o_ssem, o_rsem, x_ssem, x_rsem, y_ssem, y_rsem, c_ssem, c_rsem,
    gz_ssem, gz_rsem, gx_ssem, gx_rsem, gy_ssem, gy_rsem, gc_ssem, gc_rsem,
):
    span, width = vbuf.shape
    cw = width // nsp
    groups = cw // GD
    piece = v_piece(span)
    pieces = span // piece
    total = nsp * pieces
    tail = guest_rows(ngrp, nsp, ndp, span)
    half = (nsp + 1) // 2
    nx = ndp // 2
    rows = BLK // ndp
    part = rows // ngrp
    p, z, r = lax.axis_index("grp"), lax.axis_index("sp"), lax.axis_index("dp")
    xi, core = r // 2, r % 2
    mate = r + 1 - 2 * core
    upper = z // half

    def value_copy(i):
        at = pl.ds(i * piece, piece)
        return pltpu.make_async_copy(value_hbm.at[0, at], vbuf.at[at], v_sem.at[i])

    def own_rows(block, q, count):
        return pl.ds(pl.multiple_of(block * rows + q * part, part), count)

    mine = own_rows(r, 0, rows)
    w_copy = pltpu.make_async_copy(w_hbm, wbuf.at[:, mine], w_sem)
    gate_copy = pltpu.make_async_copy(gate_hbm.at[0], gbuf, g_sem)
    value_copy(0).start()
    w_copy.start()
    for i in range(1, pieces):
        value_copy(i).start()
    gate_copy.start()

    barrier = pltpu.get_barrier_semaphore()
    peers = [{"sp": lax.rem(z + k, nsp)} for k in range(1, nsp)]
    peers += [{"dp": mate}]
    peers += [{"dp": lax.rem(xi + k, nx) * 2 + core} for k in range(1, nx)]
    peers += [{"grp": lax.rem(p + k, ngrp)} for k in range(1, ngrp)]
    for peer in peers:
        pl.semaphore_signal(barrier, inc=1, device_id=peer, device_id_type=pl.DeviceIdType.MESH)
    pl.semaphore_wait(barrier, len(peers))

    def remote(src, dst, ssem, rsem, device):
        return pltpu.make_async_remote_copy(
            src_ref=src, dst_ref=dst, send_sem=ssem, recv_sem=rsem,
            device_id=device, device_id_type=pl.DeviceIdType.MESH,
        )

    def peer_at(j):
        return upper * j + (1 - upper) * (nsp - 1 - j)

    def kind_of(gp, c):
        if not tail:
            return 0
        return (gp * piece // BLK) * (1 - c // half)

    def at_piece(gp, kind):
        return pl.ds(pl.multiple_of(gp * piece + kind * tail, piece), piece)

    def forward(i, c, src, kind):
        return remote(
            nsend.at[c, pl.ds(i * piece, piece)], ex.at[at_piece(src * pieces + i, kind)],
            f_ssem.at[i, c], f_rsem.at[kind, i, src], {"sp": c + half * kind},
        )

    def forward_own(i, c, kind):
        return pltpu.make_async_copy(
            nsend.at[c, pl.ds(i * piece, piece)], ex.at[at_piece(z * pieces + i, kind)],
            own_sem.at[kind, i],
        )

    def each_chunk(i, remote_step, own_step):
        for j in range(nsp):
            c = peer_at(j)
            kind = kind_of(z * pieces + i, c)

            @pl.when(c + half * kind != z)
            def _(c=c, kind=kind):
                remote_step(i, c, kind)

            if own_step is not None:
                @pl.when(c + half * kind == z)
                def _(c=c, kind=kind):
                    own_step(i, c, kind)

    gain = gain_ref[...].astype(jnp.float32)
    nbias = nbias_ref[...].astype(jnp.float32)

    def normalise(i):
        def step(s, carry):
            at = pl.ds(pl.multiple_of(i * piece + s * 16, 16), 16)
            act = gelu(vbuf[at, :].astype(jnp.float32))
            mean = jnp.sum(act, axis=-1, keepdims=True) * (1.0 / width)
            act = act - mean
            var = jnp.sum(act * act, axis=-1, keepdims=True) * (1.0 / width)
            normed = (act * lax.rsqrt(var + 1e-06) * gain + nbias).astype(jnp.bfloat16)
            for t in range(nsp):
                nsend[t, at, :] = normed[:, t * cw:(t + 1) * cw]
            return carry

        lax.fori_loop(0, piece // 16, step, 0, unroll=2)

    hc = BLK // 2

    def halves(src, action):
        action(0)

        @pl.when(src >= nx // 2)
        def _():
            action(1)

    def w_own(h):
        at = wbuf.at[:, mine, pl.ds(h * hc, hc)]
        return remote(at, at, o_ssem.at[h], o_rsem.at[h], {"dp": mate})

    def w_own_in(h):
        at = wbuf.at[:, own_rows(mate, 0, rows), pl.ds(h * hc, hc)]
        return remote(at, at, o_ssem.at[h], o_rsem.at[h], {"dp": mate})

    def w_x(g, src, dest, slot, h):
        at = wbuf.at[g, own_rows(src * 2 + core, p, part), pl.ds(h * hc, hc)]
        return remote(
            at, at, x_ssem.at[slot, g, h], x_rsem.at[src, g, h], {"dp": dest * 2 + core}
        )

    def w_y(g, src, q, slot, dest, h):
        at = wbuf.at[g, own_rows(src * 2 + core, q, part), pl.ds(h * hc, hc)]
        return remote(at, at, y_ssem.at[slot, src, g, h], y_rsem.at[q, src, g, h], {"grp": dest})

    def w_c(g, src, q, side, h):
        at = wbuf.at[g, own_rows(src * 2 + side, q, part), pl.ds(h * hc, hc)]
        return remote(at, at, c_ssem.at[q, src, g, h], c_rsem.at[q, src, g, h], {"dp": mate})

    def guest_at(g, q, side):
        return wguest.at[g, own_rows(side, q, part)]

    def gz(g, dest):
        at = wbuf.at[g, own_rows(core, p, part), pl.ds(0, tail)]
        return remote(at, guest_at(g, p, core), gz_ssem.at[g], gz_rsem.at[g], {"sp": dest})

    def gx(g):
        at = guest_at(g, p, core)
        return remote(at, at, gx_ssem.at[g], gx_rsem.at[g], {"dp": (1 - xi) * 2 + core})

    def gy(g, q):
        at = guest_at(g, q, core)
        return remote(at, at, gy_ssem.at[g], gy_rsem.at[g], {"grp": 1 - p})

    def gc(g, q, side):
        at = guest_at(g, q, side)
        return remote(at, at, gc_ssem.at[q, g], gc_rsem.at[q, g], {"dp": mate})

    odd = [g for g in range(groups) if g % 2]
    even = [g for g in range(groups) if not g % 2]

    def from_x(g):
        for k in range(1, nx):
            src = lax.rem(xi + nx - k, nx)

            def pass_on(h, src=src, k=k):
                w_x(g, src, src, k - 1, h).wait_recv()
                for m in range(1, ngrp):
                    w_y(g, src, p, m - 1, lax.rem(p + m, ngrp), h).start()
                w_c(g, src, p, core, h).start()

            halves(src, pass_on)
        if tail and g % 2:
            @pl.when((upper == 0) & (xi == 1))
            def _():
                gz(g, z + half).start()

    def from_y(g):
        for k in range(1, nx):
            src = lax.rem(xi + nx - k, nx)
            for m in range(1, ngrp):
                q = lax.rem(p + ngrp - m, ngrp)

                def pass_on(h, src=src, m=m, q=q):
                    w_y(g, src, q, m - 1, q, h).wait_recv()
                    w_c(g, src, q, core, h).start()

                halves(src, pass_on)

    for i in range(pieces):
        if i == pieces - 1:
            for g in odd:
                from_x(g)
        value_copy(i).wait()
        normalise(i)
        each_chunk(
            i,
            lambda i, c, kind: forward(i, c, z, kind).start(),
            lambda i, c, kind: forward_own(i, c, kind).start(),
        )
        if i == 0:
            w_copy.wait()
            for g in odd + even:
                for k in range(1, nx):
                    halves(xi, lambda h, g=g, k=k: w_x(
                        g, xi, lax.rem(xi + k, nx), k - 1, h).start())
            halves(xi, lambda h: w_own(h).start())
            if tail:
                @pl.when((upper == 0) & (xi == 0))
                def _():
                    for g in even:
                        gz(g, z + half).start()

    gate_copy.wait()

    def gate_step(s, carry):
        at = pl.ds(pl.multiple_of(s * 16, 16), 16)
        ggelu[at, :] = gelu(gbuf[at, :].astype(jnp.float32))
        return carry

    lax.fori_loop(0, span // 16, gate_step, 0)
    for g in odd:
        from_y(g)
    for g in even:
        from_x(g)
    for g in even:
        from_y(g)

    weights_in = set()

    def need_weights(block):
        if block in weights_in:
            return
        weights_in.add(block)
        src, side = block // 2, block % 2

        @pl.when((src == xi) & (side != core))
        def _():
            for h in range(1 + (src >= nx // 2)):
                w_own_in(h).wait_recv()

        @pl.when((src != xi) & (side != core))
        def _():
            for g in range(groups):
                for q in range(ngrp):
                    for h in range(1 + (src >= nx // 2)):
                        w_c(g, src, q, side, h).wait_recv()

    ready = set()

    def need(gp, kind):
        if (gp, kind) in ready:
            return
        ready.add((gp, kind))
        src, i = gp // pieces, gp % pieces

        @pl.when(z == src)
        def _():
            forward_own(i, z - half * kind, kind).wait()

        @pl.when(z != src)
        def _():
            forward(i, z - half * kind, src, kind).wait_recv()

    def back(gp, c, kind, dest):
        at = pl.ds((gp % pieces) * piece, piece)
        return remote(
            rsend.at[at_piece(gp, kind)], ret.at[c, at],
            b_ssem.at[kind, gp], b_rsem.at[c, gp % pieces], {"sp": dest},
        )

    def back_own(gp, c, kind, i):
        return pltpu.make_async_copy(
            rsend.at[at_piece(gp, kind)], ret.at[c, pl.ds(i * piece, piece)],
            ret_own_sem.at[kind, i],
        )

    def mix(gp, kind):
        at = gp * piece
        base = at // BLK * BLK
        t0 = at - base
        for block in range(t0 // rows, (t0 + piece - 1) // rows + 1):
            if not kind:
                need_weights(block)
        for other in range(base // piece, gp + 1):
            need(other, kind)
        weights = wguest if kind else wbuf
        keep = (
            lax.broadcasted_iota(jnp.int32, (piece, piece), 1)
            <= lax.broadcasted_iota(jnp.int32, (piece, piece), 0)
        )
        lo, mid = base + kind * tail, at + kind * tail
        for g in range(groups):
            lanes = slice(g * GD, (g + 1) * GD)
            diag = weights[g, t0:t0 + piece, t0:t0 + piece]
            diag = jnp.where(keep, diag, jnp.zeros_like(diag))
            acc = jnp.dot(diag, ex[mid:mid + piece, lanes], preferred_element_type=jnp.float32)
            if t0:
                acc += jnp.dot(
                    weights[g, t0:t0 + piece, :t0], ex[lo:mid, lanes],
                    preferred_element_type=jnp.float32,
                )
            col = g + groups * kind
            acc += mbias_ref[t0:t0 + piece, col:col + 1]
            rsend[mid:mid + piece, lanes] = acc.astype(jnp.bfloat16)
        dest = gp // pieces

        @pl.when(z == dest)
        def _():
            back_own(gp, z - half * kind, kind, gp % pieces).start()

        @pl.when(z != dest)
        def _():
            back(gp, z - half * kind, kind, dest).start()

    if tail:
        first_late = BLK // piece

        @pl.when(upper == 1)
        def _():
            for gp in range(first_late, total):
                mix(gp, 0)

        late_blocks = sorted(weights_in)
        weights_in.clear()

        @pl.when(upper == 0)
        def _():
            for block in late_blocks:
                need_weights(block)

        mix(0, 0)
        mix(1, 0)

        @pl.when(upper == 1)
        def _():
            pairs = groups // 2
            near = [2 * k + xi for k in range(pairs)]
            far = [2 * k + 1 - xi for k in range(pairs)]
            for g in near:
                gz(g, z).wait_recv()
                gx(g).start()
                gy(g, p).start()
                gc(g, p, core).start()
            for g in far:
                gx(g).wait_recv()
                gy(g, p).start()
                gc(g, p, core).start()
            for g in near + far:
                gy(g, 1 - p).wait_recv()
                gc(g, 1 - p, core).start()

        mix(2, 0)

        @pl.when(upper == 1)
        def _():
            for g in range(groups):
                for q in range(ngrp):
                    gc(g, q, 1 - core).wait_recv()
            for gp in range(first_late, total):
                mix(gp, 1)

        for gp in range(3, first_late):
            mix(gp, 0)
    else:
        for gp in range(total):
            mix(gp, 0)

    def gate_out(i, c):
        lanes = pl.ds(pl.multiple_of(c * cw, GD), cw)

        def step(s, carry):
            at = pl.ds(pl.multiple_of(i * piece + s * 16, 16), 16)
            out_ref[0, at, lanes] = (
                ggelu[at, lanes] * ret[c, at, :].astype(jnp.float32)
            ).astype(jnp.bfloat16)
            return carry

        lax.fori_loop(0, piece // 16, step, 0, unroll=2)

    for i in range(pieces):
        for j in reversed(range(nsp)):
            c = peer_at(j)
            gp = z * pieces + i
            kind = kind_of(gp, c)

            @pl.when(c + half * kind == z)
            def _(gp=gp, c=c, kind=kind, i=i):
                back_own(gp, c, kind, i).wait()

            @pl.when(c + half * kind != z)
            def _(c=c, i=i):
                back(i, c, 0, c).wait_recv()

            gate_out(i, c)

    for i in range(pieces):
        each_chunk(i, lambda i, c, kind: forward(i, c, z, kind).wait_send(), None)

    def back_sent(gp, kind):
        @pl.when(z != gp // pieces)
        def _():
            back(gp, z - half * kind, kind, gp // pieces).wait_send()

    early = BLK // piece if tail else total
    for gp in range(early):
        back_sent(gp, 0)
    if tail:
        @pl.when(upper == 1)
        def _():
            for gp in range(early, total):
                back_sent(gp, 0)
                back_sent(gp, 1)
            for g in range(groups):
                gy(g, p).wait_send()
                for q in range(ngrp):
                    gc(g, q, core).wait_send()
            for k in range(groups // 2):
                gx(2 * k + xi).wait_send()

        @pl.when(upper == 0)
        def _():
            for k in range(groups // 2):
                gz(2 * k + xi, z + half).wait_send()

    halves(xi, lambda h: w_own(h).wait_send())
    for g in range(groups):
        for k in range(1, nx):
            halves(xi, lambda h: w_x(g, xi, lax.rem(xi + k, nx), k - 1, h).wait_send())
            src = lax.rem(xi + k, nx)

            def sent(h):
                for m in range(1, ngrp):
                    w_y(g, src, p, m - 1, lax.rem(p + m, ngrp), h).wait_send()
                for q in range(ngrp):
                    w_c(g, src, q, core, h).wait_send()

            halves(src, sent)


def v_piece(span):
    return 128 if span % 128 == 0 else span


def body(ngrp, nsp, ndp, gate_input, value_input, norm_gain, norm_bias, mix_weight, mix_bias):
    _, span, width = value_input.shape
    groups = mix_weight.shape[0]
    cw = groups * GD
    pieces = span // v_piece(span)
    nx = ndp // 2
    total = nsp * pieces
    tail = guest_rows(ngrp, nsp, ndp, span)
    kinds, guest = (2, tail) if tail else (1, 16)
    bias = mix_bias.astype(jnp.float32)
    if tail:
        half = nsp // 2
        shifted = lax.ppermute(bias, "sp", [(k, k + half) for k in range(half)])
        bias = jnp.concatenate([bias, shifted])
    dma = pltpu.SemaphoreType.DMA
    bf16, f32 = jnp.bfloat16, jnp.float32
    vmem, hbm = pl.BlockSpec(memory_space=pltpu.VMEM), pl.BlockSpec(memory_space=pl.ANY)
    return pl.pallas_call(
        functools.partial(kernel, ngrp, nsp, ndp),
        out_shape=jax.ShapeDtypeStruct(value_input.shape, bf16),
        in_specs=[hbm, hbm, vmem, vmem, hbm, vmem],
        out_specs=vmem,
        scratch_shapes=[
            pltpu.VMEM((span, width), bf16),
            pltpu.VMEM((span, width), bf16),
            pltpu.VMEM((span, width), f32),
            pltpu.VMEM((nsp, span, cw), bf16),
            pltpu.VMEM((nsp * span + tail, cw), bf16),
            pltpu.VMEM((nsp * span + tail, cw), bf16),
            pltpu.VMEM((nsp, span, cw), bf16),
            pltpu.VMEM((groups, BLK, BLK), bf16),
            pltpu.VMEM((groups, guest, guest), bf16),
            dma((pieces,)), dma, dma, dma((kinds, pieces)), dma((kinds, pieces)),
            dma((pieces, nsp)), dma((kinds, pieces, nsp)),
            dma((kinds, total)), dma((nsp, pieces)),
            dma((2,)), dma((2,)),
            dma((max(nx - 1, 1), groups, 2)), dma((nx, groups, 2)),
            dma((max(ngrp - 1, 1), nx, groups, 2)), dma((ngrp, nx, groups, 2)),
            dma((ngrp, nx, groups, 2)), dma((ngrp, nx, groups, 2)),
            dma((groups,)), dma((groups,)), dma((groups,)), dma((groups,)),
            dma((groups,)), dma((groups,)), dma((ngrp, groups)), dma((ngrp, groups)),
        ],
        compiler_params=pltpu.CompilerParams(
            collective_id=0, has_side_effects=True, vmem_limit_bytes=50 * 1024 * 1024
        ),
    )(
        value_input, gate_input, norm_gain[None], norm_bias[None], mix_weight,
        bias.T,
    )


def solution(mesh):
    placed = (
        P(("grp", "dp"), "sp", None),
        P(("grp", "dp"), "sp", None),
        P(),
        P(),
        P("sp", "dp", None),
        P("sp", None),
    )
    return jax.shard_map(
        functools.partial(body, mesh.shape["grp"], mesh.shape["sp"], mesh.shape["dp"]),
        mesh=mesh, in_specs=placed, out_specs=P(("grp", "dp"), "sp", None), check_vma=False,
    )
```

time: 87.3 us -> 90 us (1.031)
  the two profiles are of different devices: /device:TPU:23 before, /device:TPU:16 now
where the time goes in v2:
time: 90 us; the launch traced here: 89.8 us
  Pallas kernels  79.8 us (89%)
  local copies, waits for them, and re-layouts  4.13 us (5%)
  waiting for transfers between devices  3.85 us (4%)
  starting transfers between devices  1.28 us (1%)
    pallas_call x1, Pallas kernels, body(): pl.pallas_call(functools.partial(kernel, ngrp, nsp, ndp), out_shape=jax.S...  79.8 us
    ppermute x1, waiting for transfers between devices, body(): shifted = lax.ppermute(bias, 'sp', [(k, k + half) for k in range(half)])  3.85 us
    unnamed x3, local copies, waits for them, and re-layouts  2.55 us
  transfers between devices with their start and end apart: 1, of which 1 were waited for; matrix products, arithmetic and copies ran while one was open for 2% of the time, Pallas kernels for 0%

profile of v2, /device:TPU:16, one launch (start us, length us, event | category | flops | bytes accessed | tf_op | source)
XLA Modules:
  0.0 89.8 jit_solution(5189533581635075221)
XLA Ops:
  0.0 0.7 convert_element_type.3
  0.7 1.3 %collective-permute-start = (f32[4,1024]{1,0:T(4,128)S(1)}, f32[4,1024]{1,0:T(4,128)S(1)}, u32[]{:S(2)}, u32[]{:S(2)}) collective-permute-start(f32[4,1024]{1,0:T(4,128)S(1)} %convert_element_type.3), channel_id=1, source_target_pairs={{0,8},{4,12},{1,9},{5,13},{2,10},{6,14},{3,11},{7,15},{16,24},{20,... | collective-permute-start | bytes 49160 | tf_op jit(solution)/shard_map/ppermute | solution.py:483
  2.0 0.7 broadcast_in_dim.6.gain_ref
  2.7 0.7 broadcast_in_dim.7.nbias_ref
  3.4 3.8 %collective-permute-done = f32[4,1024]{1,0:T(4,128)S(1)} collective-permute-done((f32[4,1024]{1,0:T(4,128)S(1)}, f32[4,1024]{1,0:T(4,128)S(1)}, u32[]{:S(2)}, u32[]{:S(2)}) %collective-permute-start) | collective-permute-done | bytes 16416 | tf_op jit(solution)/shard_map/ppermute | solution.py:483
  7.2 0.2 copy.8
  7.4 0.0 copy-start
  7.5 1.4 %copy-done = bf16[1,384,2048]{2,1,0:T(8,128)(2,1)S(1)} copy-done((bf16[1,384,2048]{2,1,0:T(8,128)(2,1)S(1)}, bf16[1,384,2048]{2,1,0:T(8,128)(2,1)}, u32[]{:S(2)}) %copy-start) | copy-done | bytes 1572888
  8.9 79.8 %shard_map.64 = bf16[1,384,2048]{2,1,0:T(8,128)(2,1)S(1)} custom-call(bf16[1,384,2048]{2,1,0:T(8,128)(2,1)S(1)} %copy-done, bf16[1,384,2048]{2,1,0:T(8,128)(2,1)} %gate_hbm.1, bf16[1,2048]{1,0:T(2,128)(2,1)S(1)} %broadcast_in_dim.6.gain_ref, bf16[1,2048]{1,0:T(2,128)(2,1)S(1)} %broadcast_in_dim.7.nbias_ref, bf16[4,256,1024]{2,1,0:T(8,128)(2,1)} %w_hbm.1, ...), custom_call_target="tpu_custom_call" | custom-call | tf_op jit(solution)/shard_map/pallas_call | solution.py:488
  88.6 1.1 %copy.10 = bf16[1,384,2048]{2,1,0:T(8,128)(2,1)} copy(bf16[1,384,2048]{2,1,0:T(8,128)(2,1)S(1)} %shard_map.64) | data formatting | bytes 3145728
  (1 shorter events, 0.0 us)
Async XLA Ops:
  0.7 6.5 %collective-permute-start = (f32[4,1024]{1,0:T(4,128)S(1)}, f32[4,1024]{1,0:T(4,128)S(1)}, u32[]{:S(2)}, u32[]{:S(2)}) collective-permute-start(f32[4,1024]{1,0:T(4,128)S(1)} %convert_element_type.3), channel_id=1, source_target_pairs={{0,8},{4,12},{1,9},{5,13},{2,10},{6,14},{3,11},{7,15},{16,24},{20,... | collective-permute-start | bytes 49160 | tf_op jit(solution)/shard_map/ppermute | solution.py:483
  7.4 1.4 %copy-start = (bf16[1,384,2048]{2,1,0:T(8,128)(2,1)S(1)}, bf16[1,384,2048]{2,1,0:T(8,128)(2,1)}, u32[]{:S(2)}) copy-start(bf16[1,384,2048]{2,1,0:T(8,128)(2,1)} %value_hbm.1) | copy-start | bytes 4718596

commit v3 on v2

--- a/solution.py
+++ b/solution.py
@@ -25,11 +25,11 @@
 
 def kernel(
     ngrp, nsp, ndp, value_hbm, gate_hbm, gain_ref, nbias_ref, w_hbm, mbias_ref, out_ref,
-    vbuf, gbuf, ggelu, nsend, ex, rsend, ret, wbuf, wguest,
+    vbuf, gbuf, ggelu, nsend, ex, rsend, ret, wbuf, wguest, gbias, bcol,
     v_sem, g_sem, w_sem, own_sem, ret_own_sem,
     f_ssem, f_rsem, b_ssem, b_rsem,
     o_ssem, o_rsem, x_ssem, x_rsem, y_ssem, y_rsem, c_ssem, c_rsem,
-    gz_ssem, gz_rsem, gx_ssem, gx_rsem, gy_ssem, gy_rsem, gc_ssem, gc_rsem,
+    gz_ssem, gz_rsem, gx_ssem, gx_rsem, gy_ssem, gy_rsem, gc_ssem, gc_rsem, gb_ssem, gb_rsem,
 ):
     span, width = vbuf.shape
     cw = width // nsp
@@ -57,8 +57,8 @@
     mine = own_rows(r, 0, rows)
     w_copy = pltpu.make_async_copy(w_hbm, wbuf.at[:, mine], w_sem)
     gate_copy = pltpu.make_async_copy(gate_hbm.at[0], gbuf, g_sem)
+    w_copy.start()
     value_copy(0).start()
-    w_copy.start()
     for i in range(1, pieces):
         value_copy(i).start()
     gate_copy.start()
@@ -213,6 +213,26 @@
 
                 halves(src, pass_on)
 
+    def bias_up(dest):
+        return remote(mbias_ref, gbias, gb_ssem, gb_rsem, {"sp": dest})
+
+    if tail:
+        @pl.when(upper == 0)
+        def _():
+            bias_up(z + half).start()
+
+    w_copy.wait()
+    for g in odd + even:
+        for k in range(1, nx):
+            halves(xi, lambda h, g=g, k=k: w_x(
+                g, xi, lax.rem(xi + k, nx), k - 1, h).start())
+    halves(xi, lambda h: w_own(h).start())
+    if tail:
+        @pl.when((upper == 0) & (xi == 0))
+        def _():
+            for g in even:
+                gz(g, z + half).start()
+
     for i in range(pieces):
         if i == pieces - 1:
             for g in odd:
@@ -224,19 +244,8 @@
             lambda i, c, kind: forward(i, c, z, kind).start(),
             lambda i, c, kind: forward_own(i, c, kind).start(),
         )
-        if i == 0:
-            w_copy.wait()
-            for g in odd + even:
-                for k in range(1, nx):
-                    halves(xi, lambda h, g=g, k=k: w_x(
-                        g, xi, lax.rem(xi + k, nx), k - 1, h).start())
-            halves(xi, lambda h: w_own(h).start())
-            if tail:
-                @pl.when((upper == 0) & (xi == 0))
-                def _():
-                    for g in even:
-                        gz(g, z + half).start()
-
+
+    bcol[0] = mbias_ref[...].T
     gate_copy.wait()
 
     def gate_step(s, carry):
@@ -247,10 +256,19 @@
     lax.fori_loop(0, span // 16, gate_step, 0)
     for g in odd:
         from_y(g)
-    for g in even:
-        from_x(g)
-    for g in even:
-        from_y(g)
+
+    def rest_of_weights():
+        for g in even:
+            from_x(g)
+        for g in even:
+            from_y(g)
+
+    if tail:
+        @pl.when(xi == 1)
+        def _():
+            rest_of_weights()
+    else:
+        rest_of_weights()
 
     weights_in = set()
 
@@ -326,8 +344,7 @@
                     weights[g, t0:t0 + piece, :t0], ex[lo:mid, lanes],
                     preferred_element_type=jnp.float32,
                 )
-            col = g + groups * kind
-            acc += mbias_ref[t0:t0 + piece, col:col + 1]
+            acc += bcol[kind, t0:t0 + piece, g:g + 1]
             rsend[mid:mid + piece, lanes] = acc.astype(jnp.bfloat16)
         dest = gp // pieces
 
@@ -357,6 +374,10 @@
 
         mix(0, 0)
         mix(1, 0)
+
+        @pl.when(xi == 0)
+        def _():
+            rest_of_weights()
 
         @pl.when(upper == 1)
         def _():
@@ -383,6 +404,8 @@
             for g in range(groups):
                 for q in range(ngrp):
                     gc(g, q, 1 - core).wait_recv()
+            bias_up(z).wait_recv()
+            bcol[1] = gbias[...].T
             for gp in range(first_late, total):
                 mix(gp, 1)
 
@@ -448,6 +471,7 @@
         def _():
             for k in range(groups // 2):
                 gz(2 * k + xi, z + half).wait_send()
+            bias_up(z + half).wait_send()
 
     halves(xi, lambda h: w_own(h).wait_send())
     for g in range(groups):
@@ -477,11 +501,7 @@
     total = nsp * pieces
     tail = guest_rows(ngrp, nsp, ndp, span)
     kinds, guest = (2, tail) if tail else (1, 16)
-    bias = mix_bias.astype(jnp.float32)
-    if tail:
-        half = nsp // 2
-        shifted = lax.ppermute(bias, "sp", [(k, k + half) for k in range(half)])
-        bias = jnp.concatenate([bias, shifted])
+    bias = jnp.pad(mix_bias.astype(jnp.float32), ((0, -groups % 8), (0, 0)))
     dma = pltpu.SemaphoreType.DMA
     bf16, f32 = jnp.bfloat16, jnp.float32
     vmem, hbm = pl.BlockSpec(memory_space=pltpu.VMEM), pl.BlockSpec(memory_space=pl.ANY)
@@ -500,6 +520,8 @@
             pltpu.VMEM((nsp, span, cw), bf16),
             pltpu.VMEM((groups, BLK, BLK), bf16),
             pltpu.VMEM((groups, guest, guest), bf16),
+            pltpu.VMEM(bias.shape, f32),
+            pltpu.VMEM((kinds, BLK, bias.shape[0]), f32),
             dma((pieces,)), dma, dma, dma((kinds, pieces)), dma((kinds, pieces)),
             dma((pieces, nsp)), dma((kinds, pieces, nsp)),
             dma((kinds, total)), dma((nsp, pieces)),
@@ -508,14 +530,14 @@
             dma((max(ngrp - 1, 1), nx, groups, 2)), dma((ngrp, nx, groups, 2)),
             dma((ngrp, nx, groups, 2)), dma((ngrp, nx, groups, 2)),
             dma((groups,)), dma((groups,)), dma((groups,)), dma((groups,)),
-            dma((groups,)), dma((groups,)), dma((ngrp, groups)), dma((ngrp, groups)),
+            dma((groups,)), dma((groups,)), dma((ngrp, groups)), dma((ngrp, groups)), dma, dma,
         ],
         compiler_params=pltpu.CompilerParams(
-            collective_id=0, has_side_effects=True, vmem_limit_bytes=50 * 1024 * 1024
+            collective_id=0, has_side_effects=True, vmem_limit_bytes=62 * 1024 * 1024
         ),
     )(
         value_input, gate_input, norm_gain[None], norm_bias[None], mix_weight,
-        bias.T,
+        bias,
     )
 
 

time: 90 us -> 94.6 us (1.051)
  Pallas kernels: 79.8 us -> 87.7 us
  waiting for transfers between devices: 3.85 us -> 0 us
  starting transfers between devices: 1.28 us -> 0 us
  local copies, waits for them, and re-layouts: 4.13 us -> 5.3 us
    pallas_call x1, Pallas kernels: 79.8 us -> 87.7 us  [body(): pl.pallas_call(functools.partial(kernel, ngrp, nsp, ndp), out_shape=jax.S...]
    ppermute x1 -> x0, waiting for transfers between devices: 3.85 us -> none  [body(): shifted = lax.ppermute(bias, 'sp', [(k, k + half) for k in range(half)])]
    pad x0 -> x1, other arithmetic: none -> 1.32 us  [body(): bias = jnp.pad(mix_bias.astype(jnp.float32), ((0, -groups % 8), (0, 0)))]
    ppermute x1 -> x0, starting transfers between devices: 1.28 us -> none  [body(): shifted = lax.ppermute(bias, 'sp', [(k, k + half) for k in range(half)])]
    unnamed x3 -> x1, local copies, waits for them, and re-layouts: 2.55 us -> 2.73 us
  transfers between devices with their start and end apart: 1 -> 0, of which waited for: 1 -> 0; matrix products, arithmetic and copies ran while one was open for 2% -> 0% of each run, Pallas kernels for 0% -> 0%
where the time goes in v3:
time: 94.6 us; the launch traced here: 94.3 us
  Pallas kernels  87.7 us (93%)
  local copies, waits for them, and re-layouts  5.3 us (6%)
  other arithmetic  1.32 us (1%)
    pallas_call x1, Pallas kernels, body(): pl.pallas_call(functools.partial(kernel, ngrp, nsp, ndp), out_shape=jax.S...  87.7 us
    unnamed x1, local copies, waits for them, and re-layouts  2.73 us

profile of v3, /device:TPU:16, one launch (start us, length us, event | category | flops | bytes accessed | tf_op | source)
XLA Modules:
  0.0 94.3 jit_solution(11573422625733538610)
XLA Ops:
  0.0 1.3 %broadcast_in_dim.6.gain_ref = bf16[1,2048]{1,0:T(2,128)(2,1)} reshape(bf16[2048]{0:T(1024)(128)(2,1)} %param.8) | data formatting | bytes 8192 | tf_op jit(solution)/shard_map/broadcast_in_dim | solution.py:539
  1.3 1.3 %broadcast_in_dim.7.nbias_ref = bf16[1,2048]{1,0:T(2,128)(2,1)} reshape(bf16[2048]{0:T(1024)(128)(2,1)} %param.9) | data formatting | bytes 8192 | tf_op jit(solution)/shard_map/broadcast_in_dim | solution.py:539
  2.6 1.3 %pad_convert_fusion.mbias_ref = f32[8,1024]{1,0:T(8,128)} fusion(bf16[4,1024]{1,0:T(4,128)(2,1)} %param.11), kind=kLoop, calls=%fused_computation | loop fusion | flops 8192 | bytes 40960 | tf_op jit(solution)/shard_map/jit(_pad)/pad | solution.py:504
  3.9 87.7 %shard_map.64 = bf16[1,384,2048]{2,1,0:T(8,128)(2,1)} custom-call(bf16[1,384,2048]{2,1,0:T(8,128)(2,1)} %value_hbm.1, bf16[1,384,2048]{2,1,0:T(8,128)(2,1)} %gate_hbm.1, bf16[1,2048]{1,0:T(2,128)(2,1)} %broadcast_in_dim.6.gain_ref, bf16[1,2048]{1,0:T(2,128)(2,1)} %broadcast_in_dim.7.nbias_ref, bf16[4,256,1024]{2,1,0:T(8,128)(2,1)} %w_hbm.1, ...), custom_call_target="tpu_custom_call" | custom-call | tf_op jit(solution)/shard_map/pallas_call | solution.py:508
  91.6 2.7 %copy.8 = bf16[1,384,2048]{2,1,0:T(8,128)(2,1)} copy(bf16[1,384,2048]{2,1,0:T(8,128)(2,1)} %shard_map.64) | data formatting | bytes 3145728
